TPU v7x, 32 devices: a whole 2x2x4 slice. The times are simulated.
32 devices in a mesh: grp: 2 (over y), ra: 4 (over z), cb: 4 (over x, core).
Axes of the slice: x: 2, y: 2, z: 4, core: 2. Of those that a mesh axis runs over, the one named last changes fastest.
Arguments:
- stream: bfloat16 [256, 4096], P('grp', 'ra'), parts along dimension 0, may hold values from -180 to 180
- w_gate: float32 [2, 4096, 11264], P(None, 'ra', 'cb'), may hold values from -0.09375 to 0.09375
- w_up: float32 [2, 4096, 11264], P(None, 'ra', 'cb'), may hold values from -0.09375 to 0.09375
- w_down: float32 [2, 11264, 4096], P(None, 'cb', 'ra'), may hold values from -0.0546875 to 0.0546875
- gate_scale: float32 [2, 11264], P(None, 'cb'), may hold values from 0.5 to 2
- up_scale: float32 [2, 11264], P(None, 'cb'), may hold values from 0.5 to 2
- down_scale: float32 [2, 4096], P(None, 'ra'), may hold values from 0.5 to 2
- pre_gain: float32 [2, 4096], P(None, 'ra'), may hold values from 0.1 to 1.9
- out_gain: float32 [4096], P('ra'), may hold values from 0.1 to 1.9
Outputs:
- normed: bfloat16 [256, 4096], P('grp', 'ra'), parts along dimension 0
There are 2 independent parts, one for each index of `grp`. A program takes and returns all parts, laid end to end along the dimension named above; an argument that names none is the same for every part. Nothing has to cross between parts.
All inputs are finite; a program needn't handle non-finite values.
Results may differ from a plain program's by a relative error of at most 0.018.
Values may be sent and summed in bfloat16 or wider, within the bound.
A program may use at most 192 MiB of HBM per device.

v0:
```python
import functools

import jax
import jax.numpy as jnp
from jax import lax
from jax.experimental import pallas as pl
from jax.experimental.pallas import tpu as pltpu
from jax.sharding import PartitionSpec as P

F32, BF16 = jnp.float32, jnp.bfloat16
MESH = pl.DeviceIdType.MESH
EPS = 1e-06
WIDTH = 256
LAG = 3
PIECES = 2
UP_SLOTS = 6
FIRST = 2
DOWN_SLOTS = 12


def body(n, layers, dim, share, chunks, stream, wg, wu, wd, gs, us, ds, pg, og, out,
         wub, wdb, usem, dsem, xb, scaled, own, sums, got, hid, acc, rinv_ref, scales, ss,
         c1s, c1r, c2s, c2r, ssum, rsum, shid, rhid, sss, rss, cs, cr):
    p = lax.axis_index("ra")
    q = lax.axis_index("cb")
    core = lax.rem(q, 2)
    mate = q + 1 - 2 * core
    xmate = lax.rem(q + 2, 4)
    tokens, cols = stream.shape
    half = tokens // 2
    wide = cols // PIECES
    w = WIDTH
    total = layers * chunks

    def up_copies(t):
        l, c, k = t // chunks, lax.rem(t, chunks), lax.rem(t, UP_SLOTS)
        at = pl.ds(pl.multiple_of(c * w, w), w)
        return (pltpu.make_async_copy(wg.at[l, :, at], wub.at[k, 0], usem.at[k, 0]),
                pltpu.make_async_copy(wu.at[l, :, at], wub.at[k, 1], usem.at[k, 1]))

    def down_copy(t):
        l, c, k = t // chunks, lax.rem(t, chunks), lax.rem(t, DOWN_SLOTS)
        at = pl.ds(pl.multiple_of(c * w, w), w)
        return pltpu.make_async_copy(wd.at[l, at, :], wdb.at[k], dsem.at[k])

    for t in range(FIRST):
        for copy in up_copies(t):
            copy.start()

    barrier = pltpu.get_barrier_semaphore()
    for k in range(1, n):
        pl.semaphore_signal(barrier, inc=1, device_id={"ra": lax.rem(p + k, n)}, device_id_type=MESH)
    pl.semaphore_signal(barrier, inc=1, device_id={"cb": mate}, device_id_type=MESH)
    pl.semaphore_signal(barrier, inc=1, device_id={"cb": xmate}, device_id_type=MESH)
    pl.semaphore_wait(barrier, n + 1)

    def remote(src, dst, send, recv, **where):
        return pltpu.make_async_remote_copy(src_ref=src, dst_ref=dst, send_sem=send, recv_sem=recv,
                                            device_id=where, device_id_type=MESH)

    right, left = jnp.minimum(p + 1, n - 1), jnp.maximum(p - 1, 0)

    def sum_copy(t, c, e):
        return remote(sums.at[t, e], got.at[t, e], ssum.at[c, e], rsum.at[c, e], ra=right if e else left)

    def hid_copy(t, c, e):
        return remote(hid.at[t, e], hid.at[t, e], shid.at[c, e], rhid.at[c, e], ra=left if e else right)

    def square_copy(l, k, src):
        return remote(ss.at[l, src], ss.at[l, src], sss.at[l, k], rss.at[l, src], ra=lax.rem(p + k, n))

    def send_squares(l):
        col = jnp.zeros((tokens, 1), F32)
        for j in range(PIECES):
            x = xb[l, j].astype(F32)
            col += jnp.sum(x * x, axis=1, keepdims=True)
        eye = (lax.broadcasted_iota(jnp.int32, (tokens, tokens), 0)
               == lax.broadcasted_iota(jnp.int32, (tokens, tokens), 1))
        row = jnp.sum(jnp.where(eye, col, 0.0), axis=0, keepdims=True)
        ss[l, p] = jnp.broadcast_to(row, (8, tokens))
        for k in range(1, n):
            square_copy(l, k, p).start()

    def take_rinv(l, first, rows):
        for k in range(1, n):
            src = lax.rem(p + k, n)
            square_copy(l, k, src).wait_recv()
        row = ss[l, 0][0:1]
        for src in range(1, n):
            row = row + ss[l, src][0:1]
        pick = (lax.broadcasted_iota(jnp.int32, (rows, tokens), 0) + first
                == lax.broadcasted_iota(jnp.int32, (rows, tokens), 1))
        col = jnp.sum(jnp.where(pick, row, 0.0), axis=1, keepdims=True)
        return lax.rsqrt(col / dim + EPS)

    def end_squares(l):
        for k in range(1, n):
            square_copy(l, k, p).wait_send()

    for t in range(total):
        row, at = slice(t // chunks, t // chunks + 1), slice(t % chunks * w, (t % chunks + 1) * w)
        scales[t, 0:1] = gs[row, at]
        scales[t, 1:2] = us[row, at]
    for j in range(PIECES):
        xb[0, j] = stream[:, j * wide:(j + 1) * wide]

    def layer(l):
        send_squares(l)
        for j in range(PIECES):
            at = pl.ds(j * wide, wide)
            scaled[:, at] = (xb[l, j].astype(F32) * pg[pl.ds(l, 1), at]).astype(BF16)
        acc[...] = jnp.zeros_like(acc)

        def products(c):
            t = l * chunks + c
            k = lax.rem(t, UP_SLOTS)
            for copy in up_copies(t):
                copy.wait()

            @pl.when(t == 0)
            def _():
                @pl.loop(FIRST, min(UP_SLOTS, total))
                def _(later):
                    for copy in up_copies(later):
                        copy.start()

                @pl.loop(0, min(DOWN_SLOTS, total))
                def _(later):
                    down_copy(later).start()

            for side in range(2):
                part = jnp.dot(scaled[...], wub[k, side].astype(BF16), preferred_element_type=F32)
                for e in range(2):
                    own[c, e, :, side * w:(side + 1) * w] = part[e * share:(e + 1) * share]

            @pl.when(t + UP_SLOTS < total)
            def _():
                for copy in up_copies(t + UP_SLOTS):
                    copy.start()

            for e in range(2):
                @pl.when(p == (0 if e else n - 1))
                def _():
                    sums[t, e] = own[c, e].astype(BF16)
                    sum_copy(t, c, e).start()

        def hop(c, h):
            t = l * chunks + c
            for e in range(2):
                @pl.when(p == (h if e else n - 1 - h))
                def _():
                    sum_copy(t, c, e).wait_recv()
                    sums[t, e] = (own[c, e] + got[t, e].astype(F32)).astype(BF16)
                    sum_copy(t, c, e).start()

        def finish(c):
            @pl.when(c == 0)
            def _():
                first = jnp.where(p == 0, 0, share)
                rinv_ref[...] = jnp.broadcast_to(take_rinv(l, first, share), rinv_ref.shape)

            for e in range(2):
                @pl.when(p == (n - 1 if e else 0))
                def _():
                    activate(c, e)

        def activate(c, e):
            t = l * chunks + c
            sum_copy(t, c, e).wait_recv()
            both = own[c, e] + got[t, e].astype(F32)
            rinv = rinv_ref[:, 0:1]
            gate = both[:, 0:w] * rinv * scales[t, 0:1]
            upper = both[:, w:2 * w] * rinv * scales[t, 1:2]
            hid[t, e] = (gate / (1.0 + jnp.exp(-gate)) * upper).astype(BF16)
            hid_copy(t, c, e).start()

        def pass_on(c, k):
            t = l * chunks + c
            for e in range(2):
                @pl.when(p == (n - 1 - k if e else k))
                def _():
                    hid_copy(t, c, e).wait_recv()
                    if k < n - 1:
                        hid_copy(t, c, e).start()

        def down(c):
            t = l * chunks + c
            k = lax.rem(t, DOWN_SLOTS)
            down_copy(t).wait()
            rows = jnp.concatenate([hid[t, 0], hid[t, 1]], axis=0)
            acc[...] += jnp.dot(rows, wdb[k].astype(BF16), preferred_element_type=F32)

            @pl.when(t + DOWN_SLOTS < total)
            def _():
                down_copy(t + DOWN_SLOTS).start()

        stages = [products]
        stages += [functools.partial(hop, h=h) for h in range(1, n - 1)]
        stages += [finish]
        stages += [functools.partial(pass_on, k=k) for k in range(1, n)]

        @pl.loop(0, chunks + LAG * (len(stages) - 1))
        def _(i):
            for place, stage in enumerate(stages):
                c = i - LAG * place

                @pl.when((c >= 0) & (c < chunks))
                def _(stage=stage, c=c):
                    stage(c)
                    if place == len(stages) - 1:
                        down(c)

        def core_copy(j):
            return remote(c1s.at[l, j], c1r.at[l, j], cs.at[0, l, j], cr.at[0, l, j], cb=mate)

        def chip_copy(j):
            return remote(c2s.at[l, j], c2r.at[l, j], cs.at[1, l, j], cr.at[1, l, j], cb=xmate)

        mine = pl.ds(pl.multiple_of(core * half, half), half)
        other = pl.ds(pl.multiple_of((1 - core) * half, half), half)

        def back_copy(j, rows):
            return remote(xb.at[l + 1, j, rows], xb.at[l + 1, j, rows],
                          cs.at[2, l, j], cr.at[2, l, j], cb=mate)

        for j in range(PIECES):
            c1s[l, j] = acc[other, j * wide:(j + 1) * wide].astype(BF16)
            core_copy(j).start()
        for j in range(PIECES):
            core_copy(j).wait_recv()
            c2s[l, j] = (acc[mine, j * wide:(j + 1) * wide] + c1r[l, j].astype(F32)).astype(BF16)
            chip_copy(j).start()

        @pl.loop(0, chunks)
        def _(c):
            t = l * chunks + c
            for e in range(2):
                @pl.when(p != (n - 1 if e else 0))
                def _():
                    sum_copy(t, c, e).wait_send()

                @pl.when(p != (0 if e else n - 1))
                def _():
                    hid_copy(t, c, e).wait_send()
        end_squares(l)

        for j in range(PIECES):
            chip_copy(j).wait_recv()
            at = pl.ds(j * wide, wide)
            branch = (c2s[l, j].astype(F32) + c2r[l, j].astype(F32)) * ds[pl.ds(l, 1), at]
            xb[l + 1, j, mine] = (0.5 * xb[l, j, mine].astype(F32) + branch).astype(BF16)
            back_copy(j, mine).start()
        for j in range(PIECES):
            back_copy(j, other).wait_recv()
            core_copy(j).wait_send()
            chip_copy(j).wait_send()
            back_copy(j, mine).wait_send()

    pl.loop(0, layers)(layer)

    send_squares(layers)
    rinv = take_rinv(layers, 0, tokens)
    for j in range(PIECES):
        at = slice(j * wide, (j + 1) * wide)
        out[:, at] = (xb[layers, j].astype(F32) * rinv * og[0:1, at]).astype(BF16)
    end_squares(layers)


def fused(stream, w_gate, w_up, w_down, gate_scale, up_scale, down_scale, pre_gain, out_gain):
    n = lax.axis_size("ra")
    tokens, cols = stream.shape
    layers, _, units = w_gate.shape
    share, chunks, half, wide = tokens // 2, units // WIDTH, tokens // 2, cols // PIECES
    total = layers * chunks
    dma = pltpu.SemaphoreType.DMA
    scratch = [
        pltpu.VMEM((UP_SLOTS, 2, cols, WIDTH), F32),
        pltpu.VMEM((DOWN_SLOTS, WIDTH, cols), F32),
        dma((UP_SLOTS, 2)),
        dma((DOWN_SLOTS,)),
        pltpu.VMEM((layers + 1, PIECES, tokens, wide), BF16),
        pltpu.VMEM((tokens, cols), BF16),
        pltpu.VMEM((chunks, 2, share, 2 * WIDTH), F32),
        pltpu.VMEM((total, 2, share, 2 * WIDTH), BF16),
        pltpu.VMEM((total, 2, share, 2 * WIDTH), BF16),
        pltpu.VMEM((total, 2, share, WIDTH), BF16),
        pltpu.VMEM((tokens, cols), F32),
        pltpu.VMEM((share, 128), F32),
        pltpu.VMEM((total, 8, WIDTH), F32),
        pltpu.VMEM((layers + 1, n, 8, tokens), F32),
    ]
    scratch += [pltpu.VMEM((layers, PIECES, half, wide), BF16)] * 4
    scratch += [dma((chunks, 2))] * 4
    scratch += [dma((layers + 1, n))] * 2
    scratch += [dma((3, layers, PIECES))] * 2
    vmem, hbm = pl.BlockSpec(memory_space=pltpu.VMEM), pl.BlockSpec(memory_space=pl.ANY)
    return pl.pallas_call(
        functools.partial(body, n, layers, cols * n, share, chunks),
        out_shape=jax.ShapeDtypeStruct((tokens, cols), BF16),
        in_specs=[vmem, hbm, hbm, hbm] + [vmem] * 5,
        out_specs=vmem,
        scratch_shapes=scratch,
        compiler_params=pltpu.CompilerParams(
            collective_id=0, has_side_effects=True, vmem_limit_bytes=64 * 1024 * 1024 - 65536
        ),
    )(stream, w_gate, w_up, w_down, gate_scale, up_scale, down_scale, pre_gain, out_gain[None])


def plain(stream, w_gate, w_up, w_down, gate_scale, up_scale, down_scale, pre_gain, out_gain):
    current = stream
    tokens = stream.shape[0]
    dim = stream.shape[1] * lax.axis_size("ra")
    share = tokens // lax.axis_size("ra")
    for layer in range(w_gate.shape[0]):
        xvals = current.astype(F32)
        squares = jnp.sum(xvals * xvals, axis=1)
        scaled = (xvals * pre_gain[layer]).astype(BF16)
        gate_part = jnp.dot(scaled, w_gate[layer].astype(BF16), preferred_element_type=F32)
        up_part = jnp.dot(scaled, w_up[layer].astype(BF16), preferred_element_type=F32)
        down_local = w_down[layer].astype(BF16)
        total = lax.psum(squares, "ra")
        summed = (
            lax.psum_scatter(gate_part, "ra", scatter_dimension=0, tiled=True),
            lax.psum_scatter(up_part, "ra", scatter_dimension=0, tiled=True),
        )
        own_rows = lax.dynamic_slice_in_dim(total, lax.axis_index("ra") * share, share)
        rinv = lax.rsqrt(own_rows / dim + EPS)[:, None]
        gate = summed[0] * rinv * gate_scale[layer]
        upper = summed[1] * rinv * up_scale[layer]
        hidden = (jax.nn.silu(gate) * upper).astype(BF16)
        terms = jnp.dot(
            lax.all_gather(hidden, "ra", axis=0, tiled=True), down_local, preferred_element_type=F32
        )
        branch = lax.psum(terms.astype(BF16), "cb").astype(F32) * down_scale[layer]
        current = (0.5 * xvals + branch).astype(BF16)
    xvals = current.astype(F32)
    final_sum = lax.psum(jnp.sum(xvals * xvals, axis=1), "ra")
    rinv = lax.rsqrt(final_sum / dim + EPS)[:, None]
    return (xvals * rinv * out_gain).astype(BF16)


def local(*args):
    n = lax.axis_size("ra")
    tokens, cols = args[0].shape
    fits = (n >= 2 and tokens == 128 and n <= 8 and lax.axis_size("cb") == 4
            and args[1].shape[2] % WIDTH == 0 and cols % (128 * PIECES) == 0)
    return (fused if fits else plain)(*args)


def solution(mesh):
    placed = (
        P("grp", "ra"),
        P(None, "ra", "cb"),
        P(None, "ra", "cb"),
        P(None, "cb", "ra"),
        P(None, "cb"),
        P(None, "cb"),
        P(None, "ra"),
        P(None, "ra"),
        P("ra"),
    )
    return jax.shard_map(
        local, mesh=mesh, in_specs=placed, out_specs=P("grp", "ra"), check_vma=False
    )
```

profile of v0, /device:TPU:0, one launch (start us, length us, event | category | flops | bytes accessed | tf_op | source)
XLA Modules:
  0.0 99.9 jit_solution(13949949632549488420)
XLA Ops:
  0.0 98.2 %shard_map.91 = bf16[128,1024]{1,0:T(8,128)(2,1)} custom-call(bf16[128,1024]{1,0:T(8,128)(2,1)} %stream.1, f32[2,1024,2816]{2,1,0:T(8,128)} %wg.1, f32[2,1024,2816]{2,1,0:T(8,128)} %wu.1, f32[2,2816,1024]{2,1,0:T(8,128)} %wd.1, f32[2,2816]{1,0:T(2,128)} %gs.1, f32[2,2816]{1,0:T(2,128)} %us.1, f32[2,1024]{1,0:T(2,128)} %ds.1, f32[2,1024]{1,0:T(2,128)} %pg.1, ...), custom_call_target="tpu_custom_call" | custom-call | tf_op jit(solution)/shard_map/pallas_call | solution.py:297
  98.2 1.7 %copy.11 = bf16[128,1024]{1,0:T(8,128)(2,1)} copy(bf16[128,1024]{1,0:T(8,128)(2,1)} %shard_map.91) | data formatting | bytes 524288
where the time goes:
time: 100 us; the launch traced here: 99.9 us
  Pallas kernels  98.2 us (98%)
  local copies, waits for them, and re-layouts  1.67 us (2%)
    pallas_call x1, Pallas kernels, fused(): pl.pallas_call(functools.partial(body, n, layers, cols * n, share, chunks...  98.2 us

commit v1 on v0

v1 whole, which is shorter than its diff:
```python
import functools

import jax
import jax.numpy as jnp
from jax import lax
from jax.experimental import pallas as pl
from jax.experimental.pallas import tpu as pltpu
from jax.sharding import PartitionSpec as P

F32, BF16 = jnp.float32, jnp.bfloat16
MESH = pl.DeviceIdType.MESH
EPS = 1e-06
WIDTH = 128
PAIR = 2
GROUPS = 2
LAG = 5
ENDS = (0, 0, 0, 0)
AFTER = (2, 5, 2, 5)
UP_SLOTS = 8
DOWN_SLOTS = 8
LANES = 128


def plan(n, layers, chunks):
    phases = layers * GROUPS
    ends = [min(ENDS[s % len(ENDS)], chunks) for s in range(phases)]
    start, ready = [], []
    for s in range(phases):
        at = start[s - 1] + chunks if s else 0
        if s >= GROUPS:
            at = max(at, ready[s - GROUPS] + sum(AFTER[:3]))
        start.append(at)
        last = at + chunks - 1 + (n - 1) * LAG if ends[s] < chunks else 0
        if ends[s]:
            last = max(last, at + ends[s] - 1 + 2 * (n - 1) * LAG)
        ready.append(last)
    return ends, start, ready


def body(n, layers, dim, chunks, stream, wg, wu, wd, gs, us, ds, pg, og, out,
         ust, dst, wub, wdb, usem, dsem, xb, scaled, own, sr, sl, gr, gl, hid, acc, rinv_ref, scales, ss,
         c1s, c1r, c2s, c2r, rsend, rrecv, lsend, lrecv, hsend, hrecv, sss, rss, cs, cr):
    p = lax.axis_index("ra")
    q = lax.axis_index("cb")
    core = lax.rem(q, 2)
    mate = q + 1 - 2 * core
    xmate = lax.rem(q + 2, 4)
    w = WIDTH
    rows = stream.shape[0] // GROUPS
    half = rows // 2
    phases = layers * GROUPS
    blocks = chunks // PAIR
    total = layers * blocks
    wide = PAIR * w
    ring = own.shape[0]
    ends, start, ready = plan(n, layers, chunks)
    everything, low, high = slice(0, rows), slice(0, half), slice(half, rows)

    def up_copies(v):
        l, b, k = v // blocks, lax.rem(v, blocks), lax.rem(v, UP_SLOTS)
        at = pl.ds(pl.multiple_of(b * wide, wide), wide)
        return (pltpu.make_async_copy(wg.at[l, :, at], ust.at[k, 0], usem.at[k, 0]),
                pltpu.make_async_copy(wu.at[l, :, at], ust.at[k, 1], usem.at[k, 1]))

    def down_copy(v):
        l, b, k = v // blocks, lax.rem(v, blocks), lax.rem(v, DOWN_SLOTS)
        at = pl.ds(pl.multiple_of(b * wide, wide), wide)
        return pltpu.make_async_copy(wd.at[l, at, :], dst.at[k], dsem.at[k])

    for v in range(min(max(UP_SLOTS, DOWN_SLOTS), total)):
        if v < UP_SLOTS:
            for copy in up_copies(v):
                copy.start()
        if v < DOWN_SLOTS:
            down_copy(v).start()

    barrier = pltpu.get_barrier_semaphore()
    for k in range(1, n):
        pl.semaphore_signal(barrier, inc=1, device_id={"ra": lax.rem(p + k, n)}, device_id_type=MESH)
    pl.semaphore_signal(barrier, inc=1, device_id={"cb": mate}, device_id_type=MESH)
    pl.semaphore_signal(barrier, inc=1, device_id={"cb": xmate}, device_id_type=MESH)

    def remote(src, dst, send, recv, **where):
        return pltpu.make_async_remote_copy(src_ref=src, dst_ref=dst, send_sem=send, recv_sem=recv,
                                            device_id=where, device_id_type=MESH)

    right, left = jnp.minimum(p + 1, n - 1), jnp.maximum(p - 1, 0)

    def right_copy(t, part):
        return remote(sr.at[t, part], gr.at[t, part], rsend.at[lax.rem(t, ring)], rrecv.at[lax.rem(t, ring)], ra=right)

    def left_copy(t, part):
        return remote(sl.at[t, part], gl.at[t, part], lsend.at[lax.rem(t, ring)], lrecv.at[lax.rem(t, ring)], ra=left)

    def hid_lanes(t):
        return pl.ds(pl.multiple_of(lax.rem(t, PAIR) * w, w), w)

    def hid_copy(t, e):
        part, k = high if e else low, lax.rem(t, hsend.shape[0])
        at = hid_lanes(t)
        return remote(hid.at[t // PAIR, part, at], hid.at[t // PAIR, part, at], hsend.at[k, e], hrecv.at[k, e],
                      ra=left if e else right)

    def square_copy(l, g, k, src):
        return remote(ss.at[l, g, src], ss.at[l, g, src], sss.at[g, k], rss.at[g, src],
                      ra=lax.rem(p + k, n))

    def send_squares(l, g):
        x = xb[l, g].astype(F32)
        col = jnp.sum(x * x, axis=1, keepdims=True)
        eye = (lax.broadcasted_iota(jnp.int32, (rows, LANES), 0)
               == lax.broadcasted_iota(jnp.int32, (rows, LANES), 1))
        row = jnp.sum(jnp.where(eye, col, 0.0), axis=0, keepdims=True)
        ss[l, g, p] = jnp.broadcast_to(row, (8, LANES))
        for k in range(1, n):
            square_copy(l, g, k, p).start()

    def take_rinv(l, g):
        for k in range(1, n):
            square_copy(l, g, k, lax.rem(p + k, n)).wait_recv()
        for k in range(1, n):
            square_copy(l, g, k, p).wait_send()
        row = ss[l, g, 0][0:1]
        for src in range(1, n):
            row = row + ss[l, g, src][0:1]
        pick = (lax.broadcasted_iota(jnp.int32, (rows, LANES), 0)
                == lax.broadcasted_iota(jnp.int32, (rows, LANES), 1))
        col = jnp.sum(jnp.where(pick, row, 0.0), axis=1, keepdims=True)
        return lax.rsqrt(col / dim + EPS)

    def scale_rows(l, g):
        scaled[g] = (xb[l, g].astype(F32) * pg[pl.ds(l, 1), :]).astype(BF16)

    for g in range(GROUPS):
        xb[0, g] = stream[g * rows:(g + 1) * rows]
        scale_rows(0, g)
    for v in range(layers * chunks):
        row, at = slice(v // chunks, v // chunks + 1), slice(v % chunks * w, (v % chunks + 1) * w)
        scales[v, 0:1, 0:w] = gs[row, at]
        scales[v, 0:1, w:2 * w] = us[row, at]

    pl.semaphore_wait(barrier, n + 1)

    for g in range(GROUPS):
        send_squares(0, g)

    def locate(u):
        s = jnp.int32(0)
        first = jnp.int32(0)
        kept = jnp.int32(ends[0])
        for k in range(1, phases):
            s = jnp.where(u >= start[k], k, s)
            first = jnp.where(u >= start[k], start[k], first)
            kept = jnp.where(u >= start[k], ends[k], kept)
        c = u - first
        return s, s // GROUPS, lax.rem(s, GROUPS), c, (u >= 0) & (c < chunks), c >= kept

    def kinds(both):
        found = [(both, True)] if min(ends) < chunks else []
        return found + ([(jnp.logical_not(both), False)] if any(ends) else [])

    def products(s, l, g, c, both):
        t, b = s * chunks + c, c // PAIR
        v = l * blocks + b

        @pl.when(g == 0)
        def _():
            k = lax.rem(v, UP_SLOTS)
            for copy in up_copies(v):
                copy.wait()

            for j in range(PAIR):
                for side in range(2):
                    at = (2 * j + side) * w
                    wub[b, :, at:at + w] = ust[k, side, :, j * w:(j + 1) * w].astype(BF16)

            @pl.when(v + UP_SLOTS < total)
            def _():
                for copy in up_copies(v + UP_SLOTS):
                    copy.start()

        @pl.when(c == 0)
        def _():
            acc[g] = jnp.zeros_like(acc[g])

        o = lax.rem(t, ring)
        sums = jnp.dot(scaled[g], wub[b], preferred_element_type=F32)
        for j in range(PAIR):
            own[o + j] = sums[:, 2 * j * w:2 * (j + 1) * w]
        for kind, whole in kinds(both):
            @pl.when(kind & (p == 0))
            def _(part=everything if whole else high):
                for j in range(PAIR):
                    sr[t + j, part] = own[o + j, part].astype(BF16)
                    right_copy(t + j, part).start()

            @pl.when(kind & (p == n - 1))
            def _(part=everything if whole else low):
                for j in range(PAIR):
                    sl[t + j, part] = own[o + j, part].astype(BF16)
                    left_copy(t + j, part).start()

    def hop(h, s, l, g, c, both):
        t = s * chunks + c
        o = lax.rem(t, ring)
        for kind, whole in kinds(both):
            @pl.when(kind & (p == h))
            def _(part=everything if whole else high):
                right_copy(t, part).wait_recv()
                sr[t, part] = (own[o, part] + gr[t, part].astype(F32)).astype(BF16)
                right_copy(t, part).start()

            @pl.when(kind & (p == n - 1 - h))
            def _(part=everything if whole else low):
                left_copy(t, part).wait_recv()
                sl[t, part] = (own[o, part] + gl[t, part].astype(F32)).astype(BF16)
                left_copy(t, part).start()

    def activate(t, v, g, o, part):
        rinv = jnp.concatenate([rinv_ref[g, part]] * (w // LANES), axis=1)
        gate = own[o, part, 0:w] * rinv * scales[v, 0:1, 0:w]
        upper = own[o, part, w:2 * w] * rinv * scales[v, 0:1, w:2 * w]
        hid[t // PAIR, part, hid_lanes(t)] = (gate / (1.0 + jnp.exp(-gate)) * upper).astype(BF16)

    def finish(s, l, g, c, both):
        t, v = s * chunks + c, l * chunks + c
        o = lax.rem(t, ring)

        @pl.when(c == 0)
        def _():
            rinv_ref[g] = jnp.broadcast_to(take_rinv(l, g), (rows, LANES))

        @pl.when(both)
        def _():
            @pl.when(p == n - 1)
            def _():
                right_copy(t, everything).wait_recv()

            @pl.when(p == 0)
            def _():
                left_copy(t, everything).wait_recv()

            @pl.when(p > 0)
            def _():
                own[o] += gr[t].astype(F32)

            @pl.when(p < n - 1)
            def _():
                own[o] += gl[t].astype(F32)

            activate(t, v, g, o, everything)

        if any(ends):
            @pl.when(jnp.logical_not(both) & (p == n - 1))
            def _():
                right_copy(t, high).wait_recv()
                own[o, high] += gr[t, high].astype(F32)
                activate(t, v, g, o, high)
                hid_copy(t, 1).start()

            @pl.when(jnp.logical_not(both) & (p == 0))
            def _():
                left_copy(t, low).wait_recv()
                own[o, low] += gl[t, low].astype(F32)
                activate(t, v, g, o, low)
                hid_copy(t, 0).start()

    def pass_on(k, s, l, g, c, both):
        t = s * chunks + c
        for e in range(2):
            @pl.when(jnp.logical_not(both) & (p == (n - 1 - k if e else k)))
            def _(e=e):
                hid_copy(t, e).wait_recv()
                if k < n - 1:
                    hid_copy(t, e).start()

    def retire(s, l, g, c, both):
        t = s * chunks + c
        for kind, whole in kinds(both):
            @pl.when(kind & (p < n - 1))
            def _(part=everything if whole else high):
                right_copy(t, part).wait_send()

            @pl.when(kind & (p > 0))
            def _(part=everything if whole else low):
                left_copy(t, part).wait_send()

    def retire_hid(s, l, g, c, both):
        t = s * chunks + c

        @pl.when(jnp.logical_not(both) & (p < n - 1))
        def _():
            hid_copy(t, 0).wait_send()

        @pl.when(jnp.logical_not(both) & (p > 0))
        def _():
            hid_copy(t, 1).wait_send()

    def take_down(l, b):
        v = l * blocks + b
        k = lax.rem(v, DOWN_SLOTS)
        down_copy(v).wait()
        wdb[b] = dst[k].astype(BF16)

        @pl.when(v + DOWN_SLOTS < total)
        def _():
            down_copy(v + DOWN_SLOTS).start()

    def down(t, g, c):
        acc[g] += jnp.dot(hid[t // PAIR], wdb[c // PAIR], preferred_element_type=F32)

    mine = pl.ds(pl.multiple_of(core * half, half), half)
    other = pl.ds(pl.multiple_of((1 - core) * half, half), half)

    def core_copy(s):
        return remote(c1s.at[s], c1r.at[s], cs.at[0, lax.rem(s, GROUPS)], cr.at[0, lax.rem(s, GROUPS)], cb=mate)

    def chip_copy(s):
        return remote(c2s.at[s], c2r.at[s], cs.at[1, lax.rem(s, GROUPS)], cr.at[1, lax.rem(s, GROUPS)], cb=xmate)

    def back_copy(s, l, g, part):
        return remote(xb.at[l + 1, g, part], xb.at[l + 1, g, part], cs.at[2, g], cr.at[2, g], cb=mate)

    def to_core(s, l, g):
        c1s[s] = acc[g, other].astype(BF16)
        core_copy(s).start()

    def to_chip(s, l, g):
        core_copy(s).wait_recv()
        c2s[s] = (acc[g, mine] + c1r[s].astype(F32)).astype(BF16)
        chip_copy(s).start()

    def to_next(s, l, g):
        chip_copy(s).wait_recv()
        branch = (c2s[s].astype(F32) + c2r[s].astype(F32)) * ds[pl.ds(l, 1), :]
        xb[l + 1, g, mine] = (0.5 * xb[l, g, mine].astype(F32) + branch).astype(BF16)
        back_copy(s, l, g, mine).start()

    def begin(s, l, g):
        back_copy(s, l, g, other).wait_recv()
        send_squares(l + 1, g)

        @pl.when(l + 1 < layers)
        def _():
            scale_rows(l + 1, g)

        core_copy(s).wait_send()
        chip_copy(s).wait_send()
        back_copy(s, l, g, mine).wait_send()

    def close(s, l, g):
        @pl.when(l + 1 == layers)
        def _():
            rinv = take_rinv(layers, g)
            at = pl.ds(pl.multiple_of(g * rows, rows), rows)
            out[at, :] = (xb[layers, g].astype(F32) * rinv * og[0:1, :]).astype(BF16)

    def at_ready(i, after, stage):
        s, hit = jnp.int32(0), jnp.bool_(False)
        for k in range(phases):
            s = jnp.where(i == ready[k] + after, k, s)
            hit = hit | (i == ready[k] + after)

        @pl.when(hit)
        def _():
            stage(s, s // GROUPS, lax.rem(s, GROUPS))

    @pl.loop(0, ready[-1] + sum(AFTER) + 1)
    def _(i):
        def run(stage, offset, every=1):
            s, l, g, c, valid, both = locate(i - offset)

            @pl.when(valid & (lax.rem(c, every) == 0) if every > 1 else valid)
            def _():
                stage(s, l, g, c, both)

        for h in range(n - 2, 0, -1):
            run(functools.partial(hop, h), h * LAG)
        run(finish, (n - 1) * LAG)
        run(retire, (n - 1) * LAG)
        if any(ends):
            for k in range(1, n):
                run(functools.partial(pass_on, k), (n - 1 + k) * LAG)

        s, l, g, c, valid, both = locate(i - (n - 1) * LAG)

        last = PAIR - 1
        full = lax.rem(c, PAIR) == last

        @pl.when(valid & full & (g == 0))
        def _():
            take_down(l, c // PAIR)

        @pl.when(valid & full & both)
        def _():
            down(s * chunks + c, g, c)

        if any(ends):
            s2, _, g2, c2, valid2, both2 = locate(i - 2 * (n - 1) * LAG)

            @pl.when(valid2 & jnp.logical_not(both2) & (lax.rem(c2, PAIR) == last))
            def _():
                down(s2 * chunks + c2, g2, c2)

        after = 0
        for stage, step in zip((to_core, to_chip, to_next, begin, close), (0,) + AFTER):
            after += step
            at_ready(i, after, stage)
        run(products, 0, PAIR)
        if any(ends):
            run(retire_hid, 2 * (n - 1) * LAG + 1)


def fused(stream, w_gate, w_up, w_down, gate_scale, up_scale, down_scale, pre_gain, out_gain):
    n = lax.axis_size("ra")
    tokens, cols = stream.shape
    layers, _, units = w_gate.shape
    chunks, rows = units // WIDTH, tokens // GROUPS
    half, phases = rows // 2, layers * GROUPS
    items = phases * chunks
    blocks, wide = chunks // PAIR, PAIR * WIDTH
    ring = -(-((n - 1) * LAG + PAIR + 1) // PAIR) * PAIR
    dma = pltpu.SemaphoreType.DMA
    scratch = [
        pltpu.VMEM((UP_SLOTS, 2, cols, wide), F32),
        pltpu.VMEM((DOWN_SLOTS, wide, cols), F32),
        pltpu.VMEM((blocks, cols, 2 * wide), BF16),
        pltpu.VMEM((blocks, wide, cols), BF16),
        dma((UP_SLOTS, 2)),
        dma((DOWN_SLOTS,)),
        pltpu.VMEM((layers + 1, GROUPS, rows, cols), BF16),
        pltpu.VMEM((GROUPS, rows, cols), BF16),
        pltpu.VMEM((ring, rows, 2 * WIDTH), F32),
    ]
    scratch += [pltpu.VMEM((items, rows, 2 * WIDTH), BF16)] * 4
    scratch += [
        pltpu.VMEM((items // PAIR, rows, wide), BF16),
        pltpu.VMEM((GROUPS, rows, cols), F32),
        pltpu.VMEM((GROUPS, rows, LANES), F32),
        pltpu.VMEM((layers * chunks, 8, 2 * WIDTH), F32),
        pltpu.VMEM((layers + 1, GROUPS, n, 8, LANES), F32),
    ]
    scratch += [pltpu.VMEM((phases, half, cols), BF16)] * 4
    scratch += [dma((ring,))] * 4
    scratch += [dma((2 * ring if any(ENDS) else 1, 2))] * 2
    scratch += [dma((GROUPS, n))] * 2
    scratch += [dma((3, GROUPS))] * 2
    vmem, hbm = pl.BlockSpec(memory_space=pltpu.VMEM), pl.BlockSpec(memory_space=pl.ANY)
    return pl.pallas_call(
        functools.partial(body, n, layers, cols * n, chunks),
        out_shape=jax.ShapeDtypeStruct((tokens, cols), BF16),
        in_specs=[vmem, hbm, hbm, hbm] + [vmem] * 5,
        out_specs=vmem,
        scratch_shapes=scratch,
        compiler_params=pltpu.CompilerParams(
            collective_id=0, has_side_effects=True, vmem_limit_bytes=64 * 1024 * 1024 - 65536
        ),
    )(stream, w_gate, w_up, w_down, gate_scale, up_scale, down_scale, pre_gain, out_gain[None])


def plain(stream, w_gate, w_up, w_down, gate_scale, up_scale, down_scale, pre_gain, out_gain):
    current = stream
    tokens = stream.shape[0]
    dim = stream.shape[1] * lax.axis_size("ra")
    share = tokens // lax.axis_size("ra")
    for layer in range(w_gate.shape[0]):
        xvals = current.astype(F32)
        squares = jnp.sum(xvals * xvals, axis=1)
        scaled = (xvals * pre_gain[layer]).astype(BF16)
        gate_part = jnp.dot(scaled, w_gate[layer].astype(BF16), preferred_element_type=F32)
        up_part = jnp.dot(scaled, w_up[layer].astype(BF16), preferred_element_type=F32)
        down_local = w_down[layer].astype(BF16)
        total = lax.psum(squares, "ra")
        summed = (
            lax.psum_scatter(gate_part, "ra", scatter_dimension=0, tiled=True),
            lax.psum_scatter(up_part, "ra", scatter_dimension=0, tiled=True),
        )
        own_rows = lax.dynamic_slice_in_dim(total, lax.axis_index("ra") * share, share)
        rinv = lax.rsqrt(own_rows / dim + EPS)[:, None]
        gate = summed[0] * rinv * gate_scale[layer]
        upper = summed[1] * rinv * up_scale[layer]
        hidden = (jax.nn.silu(gate) * upper).astype(BF16)
        terms = jnp.dot(
            lax.all_gather(hidden, "ra", axis=0, tiled=True), down_local, preferred_element_type=F32
        )
        branch = lax.psum(terms.astype(BF16), "cb").astype(F32) * down_scale[layer]
        current = (0.5 * xvals + branch).astype(BF16)
    xvals = current.astype(F32)
    final_sum = lax.psum(jnp.sum(xvals * xvals, axis=1), "ra")
    rinv = lax.rsqrt(final_sum / dim + EPS)[:, None]
    return (xvals * rinv * out_gain).astype(BF16)


def local(*args):
    n = lax.axis_size("ra")
    tokens, cols = args[0].shape
    fits = (n >= 2 and tokens == 128 and n <= 8 and lax.axis_size("cb") == 4
            and args[1].shape[2] % (PAIR * WIDTH) == 0 and cols % LANES == 0)
    return (fused if fits else plain)(*args)


def solution(mesh):
    placed = (
        P("grp", "ra"),
        P(None, "ra", "cb"),
        P(None, "ra", "cb"),
        P(None, "cb", "ra"),
        P(None, "cb"),
        P(None, "cb"),
        P(None, "ra"),
        P(None, "ra"),
        P("ra"),
    )
    return jax.shard_map(
        local, mesh=mesh, in_specs=placed, out_specs=P("grp", "ra"), check_vma=False
    )
```

time: 100 us -> 92 us (0.920)
  Pallas kernels: 98.2 us -> 90.2 us
    pallas_call x1, Pallas kernels: 98.2 us -> 90.2 us  [fused(): pl.pallas_call(functools.partial(body, n, layers, cols * n, chunks), out_...]
where the time goes in v1:
time: 92 us; the launch traced here: 91.8 us
  Pallas kernels  90.2 us (98%)
  local copies, waits for them, and re-layouts  1.67 us (2%)
    pallas_call x1, Pallas kernels, fused(): pl.pallas_call(functools.partial(body, n, layers, cols * n, chunks), out_...  90.2 us

profile of v1, /device:TPU:0, one launch (start us, length us, event | category | flops | bytes accessed | tf_op | source)
XLA Modules:
  0.0 91.8 jit_solution(11085271310062035460)
XLA Ops:
  0.0 90.2 %shard_map.91 = bf16[128,1024]{1,0:T(8,128)(2,1)} custom-call(bf16[128,1024]{1,0:T(8,128)(2,1)} %stream.1, f32[2,1024,2816]{2,1,0:T(8,128)} %wg.1, f32[2,1024,2816]{2,1,0:T(8,128)} %wu.1, f32[2,2816,1024]{2,1,0:T(8,128)} %wd.1, f32[2,2816]{1,0:T(2,128)} %gs.1, f32[2,2816]{1,0:T(2,128)} %us.1, f32[2,1024]{1,0:T(2,128)} %ds.1, f32[2,1024]{1,0:T(2,128)} %pg.1, ...), custom_call_target="tpu_custom_call" | custom-call | tf_op jit(solution)/shard_map/pallas_call | solution.py:449
  90.2 1.7 %copy.11 = bf16[128,1024]{1,0:T(8,128)(2,1)} copy(bf16[128,1024]{1,0:T(8,128)(2,1)} %shard_map.91) | data formatting | bytes 524288
